TPU v7x, 32 devices: a whole 2x2x4 slice. The times are simulated.
32 devices in a mesh: sp: 8 (over z, y), tp: 4 (over x, core).
Axes of the slice: x: 2, y: 2, z: 4, core: 2. Of those that a mesh axis runs over, the one named last changes fastest.
Arguments:
- prompt: bfloat16 [4, 1536, 4096], P(None, 'sp'), may hold values from -6 to 6
- forget_weight: bfloat16 [4096, 2048], P(None, 'tp'), may hold values from -0.09375 to 0.09375
- value_weight: bfloat16 [4096, 2048], P(None, 'tp'), may hold values from -1.5 to 1.5
- lower_bound: float32 [2048], P('tp'), may hold values from 0.9 to 0.9996745
- extra_decay: float32 [4, 1536, 2048], P(None, 'sp', 'tp'), may hold values from -1.4045573 to 0
- new_token: bfloat16 [4, 4096], P(None, 'tp'), may hold values from -6 to 6
- new_query: bfloat16 [4, 2048], P(None, 'tp'), may hold values from -6 to 6
- read_gain: float32 [128], replicated, may hold values from 0.1 to 1.9
Outputs:
- state_cache: bfloat16 [128, 16, 4, 128], P('sp', 'tp')
- first_read: bfloat16 [4, 2048], P(None, 'tp')
All inputs are finite; a program needn't handle non-finite values.
Results may differ from a plain program's by a relative error of at most 0.0019.
The roundings to bfloat16 on the way count: a program that leaves them out, or rounds other values in their place, can miss the bound.
Values may be sent and summed in bfloat16 or wider, within the bound.
A program may use at most 64 MiB of HBM per device.

v0:
```python
import jax
import jax.numpy as jnp
from jax import lax
from jax.sharding import PartitionSpec as P

HD = 128


def entering(value, axis, join, neutral):
    count, mine = (lax.axis_size(axis), lax.axis_index(axis))
    pieces = lax.all_gather(value, axis)
    pieces = pieces[::-1]
    mine = count - 1 - mine
    total = jnp.full_like(value, 0) + jnp.asarray(neutral, value.dtype)

    def hop(position, total):
        longer = join(total, pieces[position])
        return jnp.where(position < mine, longer, total)

    return lax.fori_loop(0, count - 1, hop, total)


def add_terms(earlier, latter):
    return earlier + latter


def read_share(state_rows, decay_rows, key_share, query_rows, new_value):
    updated = jnp.exp(decay_rows)[..., None] * state_rows + key_share[..., None] * new_value[None]
    return jnp.sum(query_rows[..., None] * updated, axis=0)


def local(
    prompt, forget_weight, value_weight, lower_bound, extra_decay, new_token, new_query, read_gain
):
    seq_count = prompt.shape[0]
    span_len = prompt.shape[1]
    width_dev = forget_weight.shape[1]
    head_count = width_dev // HD
    log_lower = jnp.log(lower_bound)
    log_upper = jnp.log1p(-lower_bound)
    opening = 1.0 - lower_bound
    forget_pre = jnp.einsum(
        "std,dw->stw", prompt, forget_weight, preferred_element_type=jnp.float32
    ).astype(jnp.bfloat16)
    values = jnp.einsum(
        "std,dw->stw", prompt, value_weight, preferred_element_type=jnp.float32
    ).astype(jnp.bfloat16)
    forget_wide = lax.optimization_barrier(forget_pre).astype(jnp.float32)
    log_forget = jnp.logaddexp(log_lower, log_upper + jax.nn.log_sigmoid(forget_wide)) + extra_decay
    key_rows = opening * jax.nn.sigmoid(-forget_wide)
    running = jnp.cumsum(log_forget, axis=1)
    totals = running[:, -1]
    weighted = (key_rows * jnp.exp(totals[:, None] - running)).astype(jnp.bfloat16)
    weighted = weighted.reshape(seq_count, span_len, head_count, HD)
    value_rows = values.reshape(seq_count, span_len, head_count, HD)
    later_sum = entering(totals, "sp", add_terms, jnp.zeros_like(totals))
    end_scale = jnp.exp(later_sum).reshape(seq_count, head_count, HD).transpose(2, 1, 0)
    whole_token = lax.all_gather(new_token, "tp", axis=1, tiled=True)
    new_forget = lax.optimization_barrier(
        jnp.dot(whole_token, forget_weight, preferred_element_type=jnp.float32).astype(jnp.bfloat16)
    ).astype(jnp.float32)
    new_value = lax.optimization_barrier(
        jnp.dot(whole_token, value_weight, preferred_element_type=jnp.float32).astype(jnp.bfloat16)
    ).astype(jnp.float32)
    new_log = jnp.logaddexp(log_lower, log_upper + jax.nn.log_sigmoid(new_forget))
    new_key = opening * jax.nn.sigmoid(-new_forget)
    query_act = jax.nn.silu(new_query.astype(jnp.float32))
    decay_cols = new_log.reshape(seq_count, head_count, HD).transpose(2, 1, 0)
    key_cols = new_key.reshape(seq_count, head_count, HD).transpose(2, 1, 0)
    query_cols = query_act.reshape(seq_count, head_count, HD).transpose(2, 1, 0)
    value_cols = new_value.reshape(seq_count, head_count, HD).transpose(1, 0, 2)
    row_share = HD // lax.axis_size("sp")
    first_own = lax.axis_index("sp") * row_share
    block_state = jnp.einsum(
        "sthd,sthe->dhse", weighted, value_rows, preferred_element_type=jnp.float32
    )
    whole_state = lax.psum(block_state * end_scale[..., None], "sp")
    state_cache = lax.dynamic_slice_in_dim(whole_state, first_own, row_share, 0).astype(
        jnp.bfloat16
    )
    raw_read = read_share(whole_state, decay_cols, key_cols, query_cols, value_cols)
    raw_read = raw_read.transpose(1, 0, 2)
    normed = (
        raw_read
        * lax.rsqrt(jnp.mean(raw_read * raw_read, axis=-1, keepdims=True) + 1e-06)
        * read_gain
    )
    first_read = normed.reshape(seq_count, width_dev).astype(jnp.bfloat16)
    return (state_cache, first_read)


def solution(mesh):
    return jax.shard_map(
        local,
        mesh=mesh,
        in_specs=(
            P(None, "sp", None),
            P(None, "tp"),
            P(None, "tp"),
            P("tp"),
            P(None, "sp", "tp"),
            P(None, "tp"),
            P(None, "tp"),
            P(),
        ),
        out_specs=(P("sp", "tp", None, None), P(None, "tp")),
        check_vma=False,
    )
```

profile of v0, /device:TPU:0, one launch (start us, length us, event | category | flops | bytes accessed | tf_op | source)
XLA Modules:
  0.0 154.1 jit_solution(2838277091920605518)
XLA Ops:
  7.2 0.7 broadcast_subtract_fusion
  7.9 7.5 %fusion.23 = bf16[4,192,512]{2,1,0:T(8,128)(2,1)S(1)} fusion(bf16[4,192,4096]{2,1,0:T(8,128)(2,1)} %param.10, bf16[4096,512]{1,0:T(8,128)(2,1)} %param.11), kind=kOutput, calls=%fused_computation.27 | convolution fusion | flops 3221618688 | bytes 11272192 | tf_op jit(solution)/shard_map/std,dw->stw/dot_general | solution.py:42
  15.5 2.0 %add_bitcast_fusion = f32[4,512,192]{1,2,0:T(8,128)S(1)} fusion(f32[4,192,512]{2,1,0:T(8,128)S(1)} %copy-done.1, bf16[4,192,512]{2,1,0:T(8,128)(2,1)S(1)} %fusion.23, f32[512]{0:T(512)S(1)} %get-tuple-element.112, f32[512]{0:T(512)S(1)} %get-tuple-element.113), kind=kLoop, calls=%fused_computation.24 | loop fusion | flops 7471104 | bytes 3936256 | tf_op jit(solution)/shard_map/transpose
  17.4 0.2 pad.3
  17.7 1.6 %fusion.4 = f32[4,512,2,128]{1,2,3,0:T(2,128)S(1)} fusion(f32[4,512,2,128]{1,3,2,0:T(8,128)S(1)} %bitcast.83), kind=kOutput, calls=%fused_computation.6 | output fusion | flops 66584576 | bytes 4194304 | tf_op jit(solution)/shard_map/reduce-window
  19.3 0.1 reduce-window.9
  19.4 0.7 broadcast_add_fusion
  20.1 0.4 copy.21
  20.6 32.4 %all-gather = f32[32,1,512]{2,1,0:T(1,128)S(1)} all-gather(f32[4,1,512]{2,1,0:T(1,128)S(1)} %slice.19), channel_id=2, replica_groups=mesh['sp'=8,'tp'=4] {'sp'}, dimensions={0}, use_global_device_ids=true | all-gather | bytes 73728 | tf_op jit(solution)/shard_map/all_gather | solution.py:11
  52.9 0.2 reduce
  53.1 0.3 while.14
  53.4 7.4 %fusion.27 = bf16[4,24,4,8,128]{4,3,2,1,0:T(8,128)(2,1)S(1)} fusion(bf16[4,192,4096]{2,1,0:T(8,128)(2,1)} %param.10, bf16[4096,512]{1,0:T(8,128)(2,1)} %param.12), kind=kOutput, calls=%fused_computation.30 | convolution fusion | flops 3221618688 | bytes 11272192 | tf_op jit(solution)/shard_map/std,dw->stw/dot_general | solution.py:45
  60.9 2.0 %fusion.26 = f32[128,4,4,128]{0,3,2,1:T(8,128)} fusion(bf16[4,24,4,8,128]{4,3,2,1,0:T(8,128)(2,1)S(1)} %fusion.27, f32[128,4,4]{0,2,1:T(4,128)S(1)} %exponential_bitcast_fusion.1, f32[4,256,512]{2,1,0:T(8,128)S(1)} %bitcast.85, f32[4,512]{1,0:T(4,128)S(1)} %bitcast.86, bf16[4,192,512]{2,1,0:T(8,128)(2,1)S(1)} %fusion.23, f32[512]{0:T(512)S(1)} %get-tuple-element.111), kind=kOutput, calls=%fused_computation.29 | convolution fusion | flops 103677952 | bytes 4212736 | tf_op jit(solution)/shard_map/sthd,sthe->dhse/dot_general | solution.py:74
  62.9 5.2 %all_gather.7 = bf16[4,4096]{1,0:T(4,128)(2,1)S(1)} all-gather(bf16[4,1024]{1,0:T(4,128)(2,1)S(1)} %copy-done.2), channel_id=1, replica_groups=mesh['sp'=8,'tp'=4] {'tp'}, dimensions={1}, use_global_device_ids=true | all-gather | bytes 40960 | tf_op jit(solution)/shard_map/all_gather | solution.py:58
  68.1 3.2 %convolution_convert_fusion.1 = bf16[4,512]{1,0:T(4,128)(2,1)S(1)} fusion(bf16[4,4096]{1,0:T(4,128)(2,1)S(1)} %all_gather.7, bf16[4096,512]{1,0:T(8,128)(2,1)} %param.11), kind=kOutput, calls=%fused_computation.32 | convolution fusion | flops 16779264 | bytes 4231168 | tf_op jit(solution)/shard_map/dot_general | solution.py:60
  71.4 0.5 copy-done
  71.8 0.6 convolution_convert_fusion
  72.5 0.1 exponential_bitcast_fusion
  72.6 69.7 %all-reduce.3.cloned.1.call-done = f32[128,4,4,128]{0,3,2,1:T(8,128)} async-done(((f32[128,4,4,128]{0,3,2,1:T(8,128)}), f32[128,4,4,128]{0,3,2,1:T(8,128)}) %all-reduce.3.cloned.1.call-update) | async-done | bytes 1048592 | tf_op jit(solution)/shard_map/psum | solution.py:77
  142.3 1.9 %multiply_reduce_fusion = f32[4,4,128]{2,1,0:T(4,128)S(1)} fusion(f32[128,4,4,128]{0,3,2,1:T(8,128)} %all-reduce.3.cloned.1.call-done, f32[4,4,128]{2,1,0:T(4,128)S(1)} %convert_bitcast_fusion, f32[128,4,4]{0,2,1:T(4,128)S(1)} %get-tuple-element.110, f32[128,4,4]{0,2,1:T(4,128)S(1)} %get-tuple-element.109, f32[128,4,4]{0,2,1:T(4,128)S(1)} %get-tuple-element.114), kind=kLoop, calls=%fused_computation.33 | loop fusion | flops 1308672 | bytes 1089536 | tf_op jit(solution)/shard_map/reduce_sum | solution.py:29
  144.2 0.1 fusion.50
  144.3 1.4 dynamic-slice_convert_fusion
  145.7 0.8 copy.29
  146.6 0.7 fusion.53
  (28 shorter events, 0.3 us)
Async XLA Ops:
  7.2 135.2 %all-reduce.3.cloned.1.call-start = ((), (), s32[]{:S(2)}) async-start(), calls=%async_computation | async-start | bytes 2097152 | tf_op jit(solution)/shard_map/psum | solution.py:77
  7.9 7.5 %copy-start.1 = (f32[4,192,512]{2,1,0:T(8,128)S(1)}, f32[4,192,512]{2,1,0:T(8,128)}, u32[]{:S(2)}) copy-start(f32[4,192,512]{2,1,0:T(8,128)} %param.14) | copy-start | bytes 4718596
  60.9 2.1 %copy-start.2 = (bf16[4,1024]{1,0:T(4,128)(2,1)S(1)}, bf16[4,1024]{1,0:T(4,128)(2,1)}, u32[]{:S(2)}) copy-start(bf16[4,1024]{1,0:T(4,128)(2,1)} %param.15) | copy-start | bytes 24580
  68.1 3.7 %copy-start = (bf16[4096,512]{1,0:T(8,128)(2,1)S(1)}, bf16[4096,512]{1,0:T(8,128)(2,1)}, u32[]{:S(2)}) copy-start(bf16[4096,512]{1,0:T(8,128)(2,1)} %param.12) | copy-start | bytes 12582916
  71.8 0.7 copy-start.3
  72.5 74.1 %copy-start.4 = (f32[128]{0:T(128)S(1)}, f32[128]{0:T(128)}, u32[]{:S(2)}) copy-start(f32[128]{0:T(128)} %param.17) | copy-start | bytes 1540
Sparse Core Ops, SparseCore 0:
  63.0 79.2 all-reduce.2
where the time goes:
time: 154 us
  waiting for transfers between devices  69.8 us (45%)
  blocking collectives  37.5 us (24%)
  matrix products  20.8 us (14%)
  between operations  14.2 us (9%)
  other arithmetic  8.07 us (5%)
  local copies, waits for them, and re-layouts  3.48 us (2%)
    psum x1, waiting for transfers between devices, local(): whole_state = lax.psum(block_state * end_scale[..., None], 'sp')  69.7 us
    all_gather x1, blocking collectives, entering(): pieces = lax.all_gather(value, axis)  32.4 us
    dot_general x1, matrix products, local(): jnp.einsum('std,dw->stw', prompt, forget_weight, preferred_element_type=j...  7.52 us
    dot_general x1, matrix products, local(): jnp.einsum('std,dw->stw', prompt, value_weight, preferred_element_type=jn...  7.42 us
    all_gather x1, blocking collectives, local(): whole_token = lax.all_gather(new_token, 'tp', axis=1, tiled=True)  5.19 us
    dot_general x1, matrix products, local(): jnp.dot(whole_token, forget_weight, preferred_element_type=jnp.float32)  3.23 us
  transfers between devices with their start and end apart: 1, of which 1 were waited for; matrix products, arithmetic and copies ran while one was open for 3% of the time, Pallas kernels for 0%

commit v1 on v0

--- a/solution.py
+++ b/solution.py
@@ -74,7 +74,7 @@
     block_state = jnp.einsum(
         "sthd,sthe->dhse", weighted, value_rows, preferred_element_type=jnp.float32
     )
-    whole_state = lax.psum(block_state * end_scale[..., None], "sp")
+    whole_state = jnp.sum(lax.all_gather(block_state * end_scale[..., None], "sp"), axis=0)
     state_cache = lax.dynamic_slice_in_dim(whole_state, first_own, row_share, 0).astype(
         jnp.bfloat16
     )

time: 154 us -> 213 us (1.38)
  waiting for transfers between devices: 69.8 us -> 114 us
  local copies, waits for them, and re-layouts: 3.48 us -> 10.5 us
  other arithmetic: 8.07 us -> 12.6 us
  matrix products: 20.8 us -> 23.1 us
    all_gather x0 -> x1, waiting for transfers between devices: none -> 114 us  [local(): lax.all_gather(block_state * end_scale[..., None], 'sp')]
    psum x1 -> x0, waiting for transfers between devices: 69.7 us -> none  [local(): whole_state = lax.psum(block_state * end_scale[..., None], 'sp')]
    unnamed x12 -> x11, local copies, waits for them, and re-layouts: 1.36 us -> 9.54 us
    reduce_sum x0 -> x1, other arithmetic: none -> 5.61 us  [local(): jnp.sum(lax.all_gather(block_state * end_scale[..., None], 'sp'), axis=0)]
    dot_general x1, matrix products: 0.64 us -> 3.26 us  [local(): jnp.dot(whole_token, value_weight, preferred_element_type=jnp.float32)]
where the time goes in v1:
time: 213 us
  waiting for transfers between devices  114 us (54%)
  blocking collectives  37.7 us (18%)
  matrix products  23.1 us (11%)
  between operations  14.2 us (7%)
  other arithmetic  12.6 us (6%)
  local copies, waits for them, and re-layouts  10.5 us (5%)
    all_gather x1, waiting for transfers between devices, local(): lax.all_gather(block_state * end_scale[..., None], 'sp')  114 us
    all_gather x1, blocking collectives, entering(): pieces = lax.all_gather(value, axis)  32.4 us
    unnamed x11, local copies, waits for them, and re-layouts  9.54 us
    dot_general x1, matrix products, local(): jnp.einsum('std,dw->stw', prompt, forget_weight, preferred_element_type=j...  7.52 us
    dot_general x1, matrix products, local(): jnp.einsum('std,dw->stw', prompt, value_weight, preferred_element_type=jn...  7.41 us
    reduce_sum x1, other arithmetic, local(): jnp.sum(lax.all_gather(block_state * end_scale[..., None], 'sp'), axis=0)  5.61 us
    all_gather x1, blocking collectives, local(): whole_token = lax.all_gather(new_token, 'tp', axis=1, tiled=True)  5.37 us
  transfers between devices with their start and end apart: 1, of which 1 were waited for; matrix products, arithmetic and copies ran while one was open for 3% of the time, Pallas kernels for 0%

profile of v1, /device:TPU:0, one launch (start us, length us, event | category | flops | bytes accessed | tf_op | source)
XLA Modules:
  0.0 212.7 jit_solution(17090082848711890020)
XLA Ops:
  7.2 0.7 broadcast_subtract_fusion
  7.9 7.5 %fusion.23 = bf16[4,192,512]{2,1,0:T(8,128)(2,1)S(1)} fusion(bf16[4,192,4096]{2,1,0:T(8,128)(2,1)} %param.10, bf16[4096,512]{1,0:T(8,128)(2,1)} %param.11), kind=kOutput, calls=%fused_computation.27 | convolution fusion | flops 3221618688 | bytes 11272192 | tf_op jit(solution)/shard_map/std,dw->stw/dot_general | solution.py:42
  15.4 2.0 add_bitcast_fusion
  17.4 0.2 pad.3
  17.7 1.6 fusion.4
  19.4 0.7 broadcast_add_fusion
  20.1 0.4 copy.20
  20.5 32.4 %all-gather = f32[32,1,512]{2,1,0:T(1,128)S(1)} all-gather(f32[4,1,512]{2,1,0:T(1,128)S(1)} %slice.19), channel_id=2, replica_groups=mesh['sp'=8,'tp'=4] {'sp'}, dimensions={0}, use_global_device_ids=true | all-gather | bytes 73728 | tf_op jit(solution)/shard_map/all_gather | solution.py:11
  52.9 0.2 reduce
  53.1 0.3 while.14
  53.4 7.4 %fusion.27 = bf16[4,24,4,8,128]{4,3,2,1,0:T(8,128)(2,1)S(1)} fusion(bf16[4,192,4096]{2,1,0:T(8,128)(2,1)} %param.10, bf16[4096,512]{1,0:T(8,128)(2,1)} %param.12), kind=kOutput, calls=%fused_computation.30 | convolution fusion | flops 3221618688 | bytes 11272192 | tf_op jit(solution)/shard_map/std,dw->stw/dot_general | solution.py:45
  60.9 2.1 fusion.26
  63.0 5.4 %all_gather.15 = bf16[4,4096]{1,0:T(4,128)(2,1)S(1)} all-gather(bf16[4,1024]{1,0:T(4,128)(2,1)S(1)} %copy-done.1), channel_id=1, replica_groups=mesh['sp'=8,'tp'=4] {'tp'}, dimensions={1}, use_global_device_ids=true | all-gather | bytes 40960 | tf_op jit(solution)/shard_map/all_gather | solution.py:58
  68.3 2.8 %convolution_convert_fusion.1 = bf16[4,512]{1,0:T(4,128)(2,1)S(1)} fusion(bf16[4,4096]{1,0:T(4,128)(2,1)S(1)} %all_gather.15, bf16[4096,512]{1,0:T(8,128)(2,1)} %param.11), kind=kOutput, calls=%fused_computation.32 | convolution fusion | flops 16779264 | bytes 4231168 | tf_op jit(solution)/shard_map/dot_general | solution.py:60
  71.2 0.1 select_exponential_fusion
  71.3 3.3 %convolution_convert_fusion = bf16[4,512]{1,0:T(4,128)(2,1)S(1)} fusion(bf16[4,4096]{1,0:T(4,128)(2,1)S(1)} %all_gather.15, bf16[4096,512]{1,0:T(8,128)(2,1)} %param.12), kind=kOutput, calls=%fused_computation.31 | convolution fusion | flops 16779264 | bytes 4231168 | tf_op jit(solution)/shard_map/dot_general | solution.py:63
  74.6 114.3 %all-gather.4.cloned.1.call-done = f32[1024,4,4,128]{0,3,2,1:T(8,128)} async-done(((f32[128,4,4,128]{0,3,2,1:T(8,128)}), f32[1024,4,4,128]{0,3,2,1:T(8,128)}) %all-gather.4.cloned.1.call-update) | async-done | bytes 8388624 | tf_op jit(solution)/shard_map/all_gather | solution.py:77
  188.9 8.7 %copy.35 = f32[256,8,8,128]{3,2,1,0:T(8,128)} copy(f32[256,8,8,128]{3,1,2,0:T(8,128)} %bitcast.78) | data formatting | bytes 16777216
  197.6 5.6 %reduce_sum.27 = f32[128,4,4,128]{0,3,2,1:T(8,128)S(1)} reduce(f32[8,128,4,4,128]{1,0,4,3,2:T(8,128)} %bitcast.77, f32[]{:T(128)} %constant.50.clone.1), dimensions={0}, to_apply=%region_4.5 | reduce | flops 1835008 | bytes 9437188 | tf_op jit(solution)/shard_map/reduce_sum | solution.py:77
  203.2 0.7 multiply_reduce_fusion
  204.0 0.1 fusion.48
  204.1 0.2 dynamic-slice_convert_fusion
  204.3 0.8 copy.29
  205.1 0.7 fusion.51
  (36 shorter events, 0.4 us)
Async XLA Ops:
  7.2 181.8 %all-gather.4.cloned.1.call-start = ((), (), s32[]{:S(2)}) async-start(), calls=%async_computation | async-start | bytes 9437184 | tf_op jit(solution)/shard_map/all_gather | solution.py:77
  7.9 7.5 %copy-start = (f32[4,192,512]{2,1,0:T(8,128)S(1)}, f32[4,192,512]{2,1,0:T(8,128)}, u32[]{:S(2)}) copy-start(f32[4,192,512]{2,1,0:T(8,128)} %param.14) | copy-start | bytes 4718596
  60.8 2.1 copy-start.1
  71.3 3.3 %copy-start.2 = (bf16[4,512]{1,0:T(4,128)(2,1)S(1)}, bf16[4,512]{1,0:T(4,128)(2,1)}, u32[]{:S(2)}) copy-start(bf16[4,512]{1,0:T(4,128)(2,1)} %param.16) | copy-start | bytes 12292
  203.2 1.9 copy-start.3
Sparse Core Ops, SparseCore 0:
  63.1 125.8 all-gather.3
